TPU v7x, 32 devices: a whole 2x2x4 slice. The times are simulated.
32 devices in a mesh: fs: 8 (over z, x), tp: 4 (over y, core).
Axes of the slice: x: 2, y: 2, z: 4, core: 2. Of those that a mesh axis runs over, the one named last changes fastest.
Arguments:
- inputs: bfloat16 [3072, 2048], P('fs'), may hold values from -6 to 6
- queries: bfloat16 [3072, 2048], P('fs', 'tp'), may hold values from -6 to 6
- keys: bfloat16 [3072, 2048], P('fs', 'tp'), may hold values from -6 to 6
- values: bfloat16 [3072, 2048], P('fs', 'tp'), may hold values from -6 to 6
- head_cot: bfloat16 [3072, 2048], P('fs', 'tp'), may hold values from -6 to 6
- mixing: float32 [16], P('tp'), may hold values from 0.3 to 0.8
- head_gain: float32 [128], replicated, may hold values from 0.1 to 1.9
- factors: bfloat16 [2048, 2, 256], P('fs'), may hold values from -0.375 to 0.375
- moments: float32 [256, 2, 2048], P('fs', None, 'tp'), may hold values from -6 to 6
- weights: float32 [2048, 2, 2048], P('fs', None, 'tp'), may hold values from -6 to 6
Outputs:
- step: float32 [2048, 2, 2048], P('fs', None, 'tp')
- new_moments: float32 [256, 2, 2048], P('fs', None, 'tp')
- copies: bfloat16 [2048, 2, 2048], P(None, None, 'tp')
All inputs are finite; a program needn't handle non-finite values.
Results may differ from a plain program's by a relative error of at most 0.007.
Values may be sent and summed in bfloat16 or wider, within the bound.
A program may use at most 64 MiB of HBM per device.

v0:
```python
import jax
import jax.numpy as jnp
from jax import lax
from jax.sharding import PartitionSpec as P

EPS = 0.05
BETA = 0.9
RATE_BASE = 0.5


def softmax_rows(scores):
    top = jnp.max(scores, axis=-1, keepdims=True)
    expo = jnp.exp(scores - top)
    return expo / jnp.sum(expo, axis=-1, keepdims=True)


def head_grads(query, key_rows, value, upstream, weight_mix, head_gain):
    length = query.shape[0]
    head_dim = query.shape[2]
    factor = head_dim ** (-0.5)
    places = jnp.arange(length)
    causal = places[None, :] <= places[:, None]

    def probs(which):
        scores = (
            jnp.dot(query[:, which], key_rows[:, which].T, preferred_element_type=jnp.float32)
            * factor
        )
        return softmax_rows(jnp.where(causal, scores, -jnp.inf))

    first = probs(0)
    second = probs(1)
    mixed = (first - weight_mix * second).astype(jnp.bfloat16)
    output = jnp.dot(mixed, value, preferred_element_type=jnp.float32)
    inverse = lax.rsqrt(jnp.mean(output * output, axis=-1, keepdims=True) + EPS)
    scaled = head_gain * upstream.astype(jnp.float32)
    d_out = inverse * scaled - output * inverse**3 * jnp.mean(
        output * scaled, axis=-1, keepdims=True
    )
    d_out = d_out.astype(jnp.bfloat16)
    d_value = jnp.dot(mixed.T, d_out, preferred_element_type=jnp.float32).astype(jnp.bfloat16)
    d_mix = jnp.dot(d_out, value.T, preferred_element_type=jnp.float32)
    d_first = (first * (d_mix - jnp.sum(first * d_mix, axis=-1, keepdims=True))).astype(
        jnp.bfloat16
    )
    d_second = (
        -weight_mix * second * (d_mix - jnp.sum(second * d_mix, axis=-1, keepdims=True))
    ).astype(jnp.bfloat16)
    q_first = (
        jnp.dot(d_first, key_rows[:, 0], preferred_element_type=jnp.float32) * factor
    ).astype(jnp.bfloat16)
    q_second = (
        jnp.dot(d_second, key_rows[:, 1], preferred_element_type=jnp.float32) * factor
    ).astype(jnp.bfloat16)
    return (jnp.stack([q_first, q_second], axis=1).reshape(length, 2 * head_dim), d_value)


def per_device(
    inputs, queries, keys, values, head_cot, mixing, head_gain, factors, moments, weights
):
    length = inputs.shape[0]
    heads_here = mixing.shape[0]
    head_width = values.shape[1] // heads_here
    head_dim = head_width // 2
    query_heads = queries.reshape(length, heads_here, 2, head_dim).transpose(1, 0, 2, 3)
    key_heads = keys.reshape(length, heads_here, 2, head_dim).transpose(1, 0, 2, 3)
    value_heads = values.reshape(length, heads_here, head_width).transpose(1, 0, 2)
    upstream_heads = head_cot.reshape(length, heads_here, head_width).transpose(1, 0, 2)

    def one_head(pieces):
        return head_grads(pieces[0], pieces[1], pieces[2], pieces[3], pieces[4], head_gain)

    d_query, d_value = lax.map(
        one_head, (query_heads, key_heads, value_heads, upstream_heads, mixing)
    )
    d_query = d_query.transpose(1, 0, 2).reshape(length, heads_here * head_width)
    d_value = d_value.transpose(1, 0, 2).reshape(length, heads_here * head_width)
    cotangents = jnp.stack([d_query, d_value], axis=1)
    fs_count = lax.axis_size("fs")
    token_factor = (length * fs_count) ** (-0.5)
    rank_here = moments.shape[0]
    cols_here = moments.shape[2]
    factor_wide = factors.astype(jnp.float32)
    whole_factors = lax.all_gather(factors, "fs", axis=0, tiled=True)
    reduced = jnp.einsum("td,dkr->tkr", inputs, whole_factors, preferred_element_type=jnp.float32)
    reduced_upper = reduced.astype(jnp.bfloat16)
    reduced_lower = (reduced - reduced_upper.astype(jnp.float32)).astype(jnp.bfloat16)
    upper_part = jnp.einsum(
        "tkr,tke->rke", reduced_upper, cotangents, preferred_element_type=jnp.float32
    )
    lower_part = jnp.einsum(
        "tkr,tke->rke", reduced_lower, cotangents, preferred_element_type=jnp.float32
    )
    projected = lax.psum_scatter(upper_part + lower_part, "fs", scatter_dimension=0, tiled=True)
    projected = projected * token_factor
    new_moments = BETA * moments + projected
    local_sums = jnp.sum(new_moments * new_moments, axis=(0, 2))
    totals = lax.psum(local_sums, ("fs", "tp"))
    entries = rank_here * fs_count * cols_here * lax.axis_size("tp")
    rate = RATE_BASE / jnp.sqrt(1.0 + totals / entries)
    low_part = jnp.einsum(
        "dkr,rke->dke",
        factor_wide,
        lax.all_gather(new_moments, "fs", axis=0, tiled=True),
        precision=lax.Precision.HIGHEST,
    )
    step = low_part * rate[None, :, None]
    copies = lax.all_gather((weights - step).astype(jnp.bfloat16), "fs", axis=0, tiled=True)
    return (step, new_moments, copies)


def solution(mesh):
    placed = (
        P("fs", None),
        P("fs", "tp"),
        P("fs", "tp"),
        P("fs", "tp"),
        P("fs", "tp"),
        P("tp"),
        P(),
        P("fs", None, None),
        P("fs", None, "tp"),
        P("fs", None, "tp"),
    )
    return jax.shard_map(
        per_device,
        mesh=mesh,
        in_specs=placed,
        out_specs=(P("fs", None, "tp"), P("fs", None, "tp"), P(None, None, "tp")),
        check_vma=False,
    )
```

profile of v0, /device:TPU:0, one launch (start us, length us, event | category | flops | bytes accessed | tf_op | source)
XLA Modules:
  0.0 282.7 jit_solution(10454785109164463003)
XLA Ops:
  7.3 1.8 copy.46
  9.2 1.2 copy.39
  10.4 1.2 copy.40
  11.6 0.2 copy.41
  11.8 1.2 copy.42
  13.0 21.3 %while.12 = (s32[]{:T(128)}, bf16[4,384,128]{1,2,0:T(8,128)(2,1)S(1)}, bf16[4,384,128]{2,1,0:T(8,128)(2,1)}, bf16[4,384,2,64]{1,3,2,0:T(8,128)(2,1)S(1)}, bf16[4...) while((s32[]{:T(128)}, ...), condition=%wide.region_9.10_spmd, body=%wide.region_0.9_spmd.sunk | while | flops 195525504 | bytes 10978449 | solution.py:73
  13.1 0.6 dynamic_slice.47
  14.3 0.3 fusion.67
  14.6 0.1 fusion.68
  14.8 0.3 fusion.65
  15.1 0.1 fusion.66
  15.2 0.8 subtract_convert_fusion.5
  16.0 0.2 multiply_reduce_fusion.6
  16.3 1.0 fusion.71
  17.3 0.4 multiply_reduce_fusion.7
  17.7 0.3 fusion.70
  18.0 0.3 fusion.69
  18.4 0.6 dynamic_slice.47
  19.6 0.3 fusion.67
  19.9 0.1 fusion.68
  20.1 0.3 fusion.65
  20.4 0.1 fusion.66
  20.5 0.8 subtract_convert_fusion.5
  21.4 0.2 multiply_reduce_fusion.6
  21.6 1.0 fusion.71
  22.6 0.4 multiply_reduce_fusion.7
  23.0 0.3 fusion.70
  23.3 0.3 fusion.69
  23.7 0.6 dynamic_slice.47
  25.0 0.3 fusion.67
  25.3 0.1 fusion.68
  25.4 0.3 fusion.65
  25.7 0.1 fusion.66
  25.8 0.8 subtract_convert_fusion.5
  26.7 0.2 multiply_reduce_fusion.6
  26.9 1.0 fusion.71
  27.9 0.4 multiply_reduce_fusion.7
  28.4 0.3 fusion.70
  28.7 0.3 fusion.69
  29.0 0.6 dynamic_slice.47
  30.3 0.3 fusion.67
  30.7 0.3 fusion.65
  31.0 0.1 fusion.66
  31.2 0.8 subtract_convert_fusion.5
  32.0 0.2 multiply_reduce_fusion.6
  32.3 1.0 fusion.71
  33.3 0.4 multiply_reduce_fusion.7
  33.7 0.3 fusion.70
  34.0 0.3 fusion.69
  34.3 1.2 copy.45
  35.6 27.0 %all-gather.4.cloned.1.call-done = bf16[2048,2,256]{2,0,1:T(8,128)(2,1)} async-done(((bf16[256,2,256]{2,0,1:T(8,128)(2,1)}), bf16[2048,2,256]{2,0,1:T(8,128)(2,1)}) %all-gather.4.cloned.1.call-update) | async-done | bytes 2097168 | tf_op jit(solution)/shard_map/all_gather | solution.py:84
  62.6 2.6 fusion.30
  65.2 0.4 fusion.35
  65.6 0.4 fusion.32
  66.1 1.3 copy.47
  67.5 0.6 dynamic-slice
  68.7 75.5 %all-reduce.3.cloned.1.call-done = f32[256,2,512]{2,1,0:T(2,128)} async-done(((f32[256,2,512]{2,1,0:T(2,128)}), f32[256,2,512]{2,1,0:T(2,128)}) %all-reduce.3.cloned.1.call-update) | async-done | bytes 1048592
  144.3 1.8 multiply_reduce_fusion.3
  146.1 1.4 copy.50
  147.6 39.7 %psum.7 = f32[2]{0:T(128)S(1)} all-reduce(f32[2]{0:T(128)S(1)} %get-tuple-element.111), channel_id=1, replica_groups=mesh['fs'=8,'tp'=4] {'fs','tp'}, use_global_device_ids=true, to_apply=%region_12.13 | all-reduce | flops 2 | bytes 16 | tf_op jit(solution)/shard_map/psum | solution.py:98
  187.3 3.5 %subtract_convert_fusion.1 = (bf16[256,2,512]{0,2,1:T(8,128)(2,1)}, f32[256,2,512]{0,2,1:T(8,128)S(1)}) fusion(f32[256,2,512]{0,2,1:T(8,128)} %copy.50, f32[2]{0:T(128)S(1)} %rsqrt_multiply_fusion, bf16[256,2,256]{2,1,0:T(2,128)(2,1)S(1)} %copy-done.1, f32[256,2,512]{2,1,0:T(2,128)} %all-gather.6.cloned.1.call-done), kind=kOutput, calls=%fused_computation.61 | convolution fusion | flops 806092800 | bytes 3932168 | tf_op jit(solution)/shard_map/dkr,rke->dke/dot_general | solution.py:101
  190.8 1.3 copy.51
  192.1 72.9 %all-gather.8.cloned.1.call-done = bf16[2048,2,512]{0,2,1:T(8,128)(2,1)} async-done(((bf16[256,2,512]{0,2,1:T(8,128)(2,1)}), bf16[2048,2,512]{0,2,1:T(8,128)(2,1)}) %all-gather.8.cloned.1.call-update) | async-done | bytes 4194320 | tf_op jit(solution)/shard_map/all_gather | solution.py:108
  265.0 11.1 %copy.52 = bf16[2048,2,512]{2,1,0:T(2,128)(2,1)} copy(bf16[2048,2,512]{0,2,1:T(8,128)(2,1)} %all-gather.8.cloned.1.call-done) | data formatting | bytes 8388608
  (49 shorter events, 0.7 us)
Async XLA Ops:
  7.2 55.4 %copy-start = (bf16[384,2048]{1,0:T(8,128)(2,1)S(1)}, bf16[384,2048]{1,0:T(8,128)(2,1)}, u32[]{:S(2)}) copy-start(bf16[384,2048]{1,0:T(8,128)(2,1)} %param.12) | copy-start | bytes 4718596
  7.2 4.4 %copy-start.3 = (bf16[384,512]{1,0:T(8,128)(2,1)S(1)}, bf16[384,512]{1,0:T(8,128)(2,1)}, u32[]{:S(2)}) copy-start(bf16[384,512]{1,0:T(8,128)(2,1)} %param.15) | copy-start | bytes 1179652
  7.2 5.8 %copy-start.5 = (f32[128]{0:T(128)S(1)}, f32[128]{0:T(128)}, u32[]{:S(2)}) copy-start(f32[128]{0:T(128)} %param.18) | copy-start | bytes 1540
  7.2 5.8 %copy-start.6 = (f32[4]{0:T(128)S(1)}, f32[4]{0:T(128)}, u32[]{:S(2)}) copy-start(f32[4]{0:T(128)} %param.17) | copy-start | bytes 52
  7.2 55.4 %all-gather.4.cloned.1.call-start = ((), (), s32[]{:S(2)}) async-start(), calls=%async_computation | async-start | bytes 2359296 | tf_op jit(solution)/shard_map/all_gather | solution.py:84
  9.1 135.2 %all-reduce.3.cloned.1.call-start = ((), (), s32[]{:S(2)}) async-start(), calls=%async_computation.3 | async-start | bytes 2097152
  66.1 1.4 copy-start.7
  66.1 78.2 %copy-start.4 = (f32[32,2,512]{2,1,0:T(2,128)S(1)}, f32[32,2,512]{2,1,0:T(2,128)}, u32[]{:S(2)}) copy-start(f32[32,2,512]{2,1,0:T(2,128)} %param.20) | copy-start | bytes 393220
  67.4 78.8 %copy-start.2 = (f32[256,2,512]{2,1,0:T(2,128)S(1)}, f32[256,2,512]{2,1,0:T(2,128)}, u32[]{:S(2)}) copy-start(f32[256,2,512]{2,1,0:T(2,128)} %param.21) | copy-start | bytes 3145732
  67.4 119.9 %copy-start.1 = (bf16[256,2,256]{2,1,0:T(2,128)(2,1)S(1)}, bf16[256,2,256]{2,1,0:T(2,128)(2,1)}, u32[]{:S(2)}) copy-start(bf16[256,2,256]{2,1,0:T(2,128)(2,1)} %param.19) | copy-start | bytes 786436
  67.4 119.9 %all-gather.6.cloned.1.call-start = ((), (), s32[]{:S(2)}) async-start(), calls=%async_computation.1 | async-start | bytes 1179648 | tf_op jit(solution)/shard_map/all_gather | solution.py:104
  146.1 118.9 %all-gather.8.cloned.1.call-start = ((), (), s32[]{:S(2)}) async-start(), calls=%async_computation.2 | async-start | bytes 4718592 | tf_op jit(solution)/shard_map/all_gather | solution.py:108
Sparse Core Ops, SparseCore 0:
  10.8 51.7 all-gather.3
  67.5 76.6 all-reduce.2
  147.0 40.0 all-gather.5
  190.9 74.0 all-gather.7
where the time goes:
time: 283 us
  waiting for transfers between devices  176 us (62%)
  blocking collectives  39.7 us (14%)
  local copies, waits for them, and re-layouts  25.2 us (9%)
  matrix products  18.3 us (6%)
  between operations  14.6 us (5%)
  other arithmetic  6.28 us (2%)
    unnamed x5, waiting for transfers between devices  75.6 us
    all_gather x1, waiting for transfers between devices, per_device(): lax.all_gather((weights - step).astype(jnp.bfloat16), 'fs', axis=0, tiled...  72.9 us
    psum x1, blocking collectives, per_device(): totals = lax.psum(local_sums, ('fs', 'tp'))  39.7 us
    all_gather x1, waiting for transfers between devices, per_device(): whole_factors = lax.all_gather(factors, 'fs', axis=0, tiled=True)  27 us
    unnamed x25, local copies, waits for them, and re-layouts  20.1 us
  transfers between devices with their start and end apart: 4, of which 3 were waited for; matrix products, arithmetic and copies ran while one was open for 10% of the time, Pallas kernels for 0%

commit v1 on v0

--- a/solution.py
+++ b/solution.py
@@ -81,8 +81,38 @@
     rank_here = moments.shape[0]
     cols_here = moments.shape[2]
     factor_wide = factors.astype(jnp.float32)
-    whole_factors = lax.all_gather(factors, "fs", axis=0, tiled=True)
-    reduced = jnp.einsum("td,dkr->tkr", inputs, whole_factors, preferred_element_type=jnp.float32)
+    length_2, index, extent = (lax.axis_size("fs"), lax.axis_index("fs"), factors.shape[0])
+    ahead = [(i, (i + 1) % length_2) for i in range(length_2)]
+    left = [(i, (i - 1) % length_2) for i in range(length_2)]
+    middle = length_2 // 2
+    from_left = from_right = factors
+    running = jnp.einsum(
+        "td,dkr->tkr",
+        lax.dynamic_slice_in_dim(inputs, index * extent, factors.shape[0], axis=1),
+        factors,
+        preferred_element_type=jnp.float32,
+    )
+    for lap in range(1, middle + 1):
+        from_left = lax.ppermute(from_left, "fs", ahead)
+        if lap < length_2 - middle:
+            from_right = lax.ppermute(from_right, "fs", left)
+            running = running + jnp.einsum(
+                "td,dkr->tkr",
+                lax.dynamic_slice_in_dim(
+                    inputs, (index + lap) % length_2 * extent, from_right.shape[0], axis=1
+                ),
+                from_right,
+                preferred_element_type=jnp.float32,
+            )
+        running = running + jnp.einsum(
+            "td,dkr->tkr",
+            lax.dynamic_slice_in_dim(
+                inputs, (index - lap) % length_2 * extent, from_left.shape[0], axis=1
+            ),
+            from_left,
+            preferred_element_type=jnp.float32,
+        )
+    reduced = running
     reduced_upper = reduced.astype(jnp.bfloat16)
     reduced_lower = (reduced - reduced_upper.astype(jnp.float32)).astype(jnp.bfloat16)
     upper_part = jnp.einsum(

time: 283 us -> 299 us (1.057)
  starting transfers between devices: 0.16 us -> 16.8 us
  waiting for transfers between devices: 176 us -> 172 us
    all_gather x1 -> x0, waiting for transfers between devices: 27 us -> none  [per_device(): whole_factors = lax.all_gather(factors, 'fs', axis=0, tiled=True)]
    ppermute x0 -> x7, waiting for transfers between devices: none -> 23.1 us  [the longest x4 20.3 us: per_device(): from_left = lax.ppermute(from_left, 'fs', ahead)]
    ppermute x0 -> x7, starting transfers between devices: none -> 16.7 us  [the longest x3 16.7 us: per_device(): from_right = lax.ppermute(from_right, 'fs', left)]
    unnamed x25 -> x29, local copies, waits for them, and re-layouts: 20.1 us -> 19.2 us
    unnamed x5 -> x4, waiting for transfers between devices: 75.6 us -> 75.6 us
  transfers between devices with their start and end apart: 4 -> 10, of which waited for: 3 -> 5; matrix products, arithmetic and copies ran while one was open for 10% -> 11% of each run, Pallas kernels for 0% -> 0%
where the time goes in v1:
time: 299 us
  waiting for transfers between devices  172 us (58%)
  blocking collectives  39.7 us (13%)
  local copies, waits for them, and re-layouts  27 us (9%)
  matrix products  19.8 us (7%)
  starting transfers between devices  16.8 us (6%)
  between operations  14.7 us (5%)
  other arithmetic  6.31 us (2%)
    unnamed x4, waiting for transfers between devices  75.6 us
    all_gather x1, waiting for transfers between devices, per_device(): lax.all_gather((weights - step).astype(jnp.bfloat16), 'fs', axis=0, tiled...  72.9 us
    psum x1, blocking collectives, per_device(): totals = lax.psum(local_sums, ('fs', 'tp'))  39.7 us
    ppermute x4, waiting for transfers between devices, per_device(): from_left = lax.ppermute(from_left, 'fs', ahead)  20.3 us
    unnamed x29, local copies, waits for them, and re-layouts  19.2 us
    ppermute x3, starting transfers between devices, per_device(): from_right = lax.ppermute(from_right, 'fs', left)  16.7 us
  transfers between devices with their start and end apart: 10, of which 5 were waited for; matrix products, arithmetic and copies ran while one was open for 11% of the time, Pallas kernels for 0%

profile of v1, /device:TPU:0, one launch (start us, length us, event | category | flops | bytes accessed | tf_op | source)
XLA Modules:
  0.0 298.7 jit_solution(14896907841881317486)
XLA Ops:
  7.2 1.8 copy.50
  9.1 6.0 %collective-permute-start = (bf16[256,2,256]{2,0,1:T(8,128)(2,1)}, bf16[256,2,256]{2,0,1:T(8,128)(2,1)}, u32[]{:S(2)}, u32[]{:S(2)}) collective-permute-start(bf16[256,2,256]{2,0,1:T(8,128)(2,1)} %copy.50), channel_id=1, source_target_pairs={{0,28},{4,0},{8,4},{12,8},{16,12},{20,16},{24,20},{28,24},{1,29},{... | collective-permute-start | bytes 786440 | tf_op jit(solution)/shard_map/ppermute | solution.py:98
  15.1 1.2 copy.43
  16.8 1.2 copy.46
  18.0 24.0 %while.12 = (s32[]{:T(128)}, bf16[4,384,128]{1,2,0:T(8,128)(2,1)}, bf16[4,384,128]{2,1,0:T(8,128)(2,1)}, bf16[4,384,2,64]{1,3,2,0:T(8,128)(2,1)S(1)}, bf16[4,384...) while((s32[]{:T(128)}, bf16[4,384,128]{1,2,0:T(8,128)(2,1)}, ...), condition=%wide.region_9.10_spmd, body=%wide.region_0.9_spmd.sunk | while | flops 195525504 | bytes 10978449 | solution.py:73
  18.0 0.7 dynamic_slice.111
  19.3 0.3 fusion.101
  19.8 0.3 fusion.99
  20.2 0.8 subtract_convert_fusion.5
  21.3 1.0 fusion.105
  22.3 0.4 multiply_reduce_fusion.7
  22.8 0.3 fusion.104
  23.1 0.3 fusion.103
  23.4 0.7 constant_dynamic-update-slice_fusion.2
  24.0 0.6 dynamic_slice.111
  25.4 0.3 fusion.101
  25.8 0.3 fusion.99
  26.2 0.8 subtract_convert_fusion.5
  27.3 1.0 fusion.105
  28.3 0.4 multiply_reduce_fusion.7
  28.8 0.3 fusion.104
  29.1 0.3 fusion.103
  29.4 0.7 constant_dynamic-update-slice_fusion.2
  30.0 0.6 dynamic_slice.111
  31.3 0.3 fusion.101
  31.8 0.3 fusion.99
  32.2 0.8 subtract_convert_fusion.5
  33.3 1.0 fusion.105
  34.3 0.4 multiply_reduce_fusion.7
  34.8 0.3 fusion.104
  35.0 0.3 fusion.103
  35.4 0.7 constant_dynamic-update-slice_fusion.2
  36.0 0.6 dynamic_slice.111
  37.3 0.3 fusion.101
  37.8 0.3 fusion.99
  38.2 0.8 subtract_convert_fusion.5
  39.3 1.0 fusion.105
  40.3 0.4 multiply_reduce_fusion.7
  40.8 0.3 fusion.104
  41.0 0.3 fusion.103
  41.4 0.7 constant_dynamic-update-slice_fusion.2
  42.0 1.2 copy.49
  43.6 4.8 %collective-permute-start.2 = (bf16[256,2,256]{2,0,1:T(8,128)(2,1)}, bf16[256,2,256]{2,0,1:T(8,128)(2,1)S(1)}, u32[]{:S(2)}, u32[]{:S(2)}) collective-permute-start(bf16[256,2,256]{2,0,1:T(8,128)(2,1)} %collective-permute-done), channel_id=1, source_target_pairs={{0,28},{4,0},{8,4},{12,8},{16,12},{20,16},{24,20},{28,24},{1,29},{... | collective-permute-start | bytes 786440 | tf_op jit(solution)/shard_map/ppermute | solution.py:98
  48.4 1.2 convolution_add_fusion.5
  49.6 1.2 convolution_add_fusion.4
  50.8 2.8 collective-permute-done.2
  53.7 5.9 %collective-permute-start.4 = (bf16[256,2,256]{2,0,1:T(8,128)(2,1)S(1)}, bf16[256,2,256]{2,0,1:T(8,128)(2,1)S(1)}, u32[]{:S(2)}, u32[]{:S(2)}) collective-permute-start(bf16[256,2,256]{2,0,1:T(8,128)(2,1)S(1)} %collective-permute-done.2), channel_id=1, source_target_pairs={{0,28},{4,0},{8,4},{12,8},{16,12},{20,16},{24,20},{28,24},{1,29},{... | collective-permute-start | bytes 786440 | tf_op jit(solution)/shard_map/ppermute | solution.py:98
  59.6 0.3 fusion.40
  59.8 0.3 fusion.33
  60.1 9.6 %collective-permute-done.5 = bf16[256,2,256]{2,0,1:T(8,128)(2,1)S(1)} collective-permute-done((bf16[256,2,256]{2,0,1:T(8,128)(2,1)S(1)}, bf16[256,2,256]{2,0,1:T(8,128)(2,1)S(1)}, u32[]{:S(2)}, u32[]{:S(2)}) %collective-permute-start.5) | collective-permute-done | bytes 262176 | tf_op jit(solution)/shard_map/ppermute | solution.py:96
  70.0 0.3 fusion.32
  70.3 10.6 %collective-permute-done.6 = bf16[256,2,256]{2,0,1:T(8,128)(2,1)S(1)} collective-permute-done((bf16[256,2,256]{2,0,1:T(8,128)(2,1)S(1)}, bf16[256,2,256]{2,0,1:T(8,128)(2,1)S(1)}, u32[]{:S(2)}, u32[]{:S(2)}) %collective-permute-start.6) | collective-permute-done | bytes 262176 | tf_op jit(solution)/shard_map/ppermute | solution.py:96
  81.2 0.4 fusion.35
  81.7 0.4 fusion.30
  82.1 1.3 copy.53
  83.5 0.6 dynamic-slice
  84.8 75.5 %all-reduce.3.cloned.1.call-done = f32[256,2,512]{2,1,0:T(2,128)} async-done(((f32[256,2,512]{2,1,0:T(2,128)}), f32[256,2,512]{2,1,0:T(2,128)}) %all-reduce.3.cloned.1.call-update) | async-done | bytes 1048592
  160.3 1.8 multiply_reduce_fusion.3
  162.2 1.4 copy.56
  163.6 39.7 %psum.7 = f32[2]{0:T(128)S(1)} all-reduce(f32[2]{0:T(128)S(1)} %get-tuple-element.111), channel_id=1, replica_groups=mesh['fs'=8,'tp'=4] {'fs','tp'}, use_global_device_ids=true, to_apply=%region_12.13 | all-reduce | flops 2 | bytes 16 | tf_op jit(solution)/shard_map/psum | solution.py:128
  203.4 3.4 %subtract_convert_fusion.1 = (bf16[256,2,512]{0,2,1:T(8,128)(2,1)}, f32[256,2,512]{0,2,1:T(8,128)S(1)}) fusion(f32[256,2,512]{0,2,1:T(8,128)} %copy.56, f32[2]{0:T(128)S(1)} %rsqrt_multiply_fusion, bf16[256,2,256]{2,1,0:T(2,128)(2,1)S(1)} %copy-done.1, f32[256,2,512]{2,1,0:T(2,128)} %all-gather.3.cloned.1.call-done), kind=kOutput, calls=%fused_computation.66 | convolution fusion | flops 806092800 | bytes 3932168 | tf_op jit(solution)/shard_map/dkr,rke->dke/dot_general | solution.py:131
  206.8 1.3 copy.57
  208.1 72.9 %all-gather.5.cloned.1.call-done = bf16[2048,2,512]{0,2,1:T(8,128)(2,1)} async-done(((bf16[256,2,512]{0,2,1:T(8,128)(2,1)}), bf16[2048,2,512]{0,2,1:T(8,128)(2,1)}) %all-gather.5.cloned.1.call-update) | async-done | bytes 4194320 | tf_op jit(solution)/shard_map/all_gather | solution.py:138
  281.0 11.1 %copy.58 = bf16[2048,2,512]{2,1,0:T(2,128)(2,1)} copy(bf16[2048,2,512]{0,2,1:T(8,128)(2,1)} %all-gather.5.cloned.1.call-done) | data formatting | bytes 8388608
  (71 shorter events, 3.7 us)
Async XLA Ops:
  7.2 36.1 %copy-start = (bf16[384,2048]{1,0:T(8,128)(2,1)S(1)}, bf16[384,2048]{1,0:T(8,128)(2,1)}, u32[]{:S(2)}) copy-start(bf16[384,2048]{1,0:T(8,128)(2,1)} %param.12) | copy-start | bytes 4718596
  7.2 9.1 %copy-start.4 = (bf16[384,512]{1,0:T(8,128)(2,1)S(1)}, bf16[384,512]{1,0:T(8,128)(2,1)}, u32[]{:S(2)}) copy-start(bf16[384,512]{1,0:T(8,128)(2,1)} %param.14) | copy-start | bytes 1179652
  7.2 9.4 %copy-start.5 = (bf16[384,512]{1,0:T(8,128)(2,1)S(1)}, bf16[384,512]{1,0:T(8,128)(2,1)}, u32[]{:S(2)}) copy-start(bf16[384,512]{1,0:T(8,128)(2,1)} %param.15) | copy-start | bytes 1179652
  7.2 153.1 %all-reduce.3.cloned.1.call-start = ((), (), s32[]{:S(2)}) async-start(), calls=%async_computation.2 | async-start | bytes 2097152
  9.1 34.5 %collective-permute-start = (bf16[256,2,256]{2,0,1:T(8,128)(2,1)}, bf16[256,2,256]{2,0,1:T(8,128)(2,1)}, u32[]{:S(2)}, u32[]{:S(2)}) collective-permute-start(bf16[256,2,256]{2,0,1:T(8,128)(2,1)} %copy.50), channel_id=1, source_target_pairs={{0,28},{4,0},{8,4},{12,8},{16,12},{20,16},{24,20},{28,24},{1,29},{... | collective-permute-start | bytes 786440 | tf_op jit(solution)/shard_map/ppermute | solution.py:98
  15.1 33.3 %collective-permute-start.1 = (bf16[256,2,256]{2,0,1:T(8,128)(2,1)}, bf16[256,2,256]{2,0,1:T(8,128)(2,1)}, u32[]{:S(2)}, u32[]{:S(2)}) collective-permute-start(bf16[256,2,256]{2,0,1:T(8,128)(2,1)} %copy.50), channel_id=1, source_target_pairs={{0,4},{4,8},{8,12},{12,16},{16,20},{20,24},{24,28},{28,0},{1,5},{5... | collective-permute-start | bytes 786440 | tf_op jit(solution)/shard_map/ppermute | solution.py:96
  15.1 2.9 copy-start.7
  15.1 2.9 copy-start.8
  18.0 25.3 %copy-start.1 = (bf16[256,2,256]{2,1,0:T(2,128)(2,1)S(1)}, bf16[256,2,256]{2,1,0:T(2,128)(2,1)}, u32[]{:S(2)}) copy-start(bf16[256,2,256]{2,1,0:T(2,128)(2,1)} %param.19) | copy-start | bytes 786436
  43.6 10.1 %collective-permute-start.2 = (bf16[256,2,256]{2,0,1:T(8,128)(2,1)}, bf16[256,2,256]{2,0,1:T(8,128)(2,1)S(1)}, u32[]{:S(2)}, u32[]{:S(2)}) collective-permute-start(bf16[256,2,256]{2,0,1:T(8,128)(2,1)} %collective-permute-done), channel_id=1, source_target_pairs={{0,28},{4,0},{8,4},{12,8},{16,12},{20,16},{24,20},{28,24},{1,29},{... | collective-permute-start | bytes 786440 | tf_op jit(solution)/shard_map/ppermute | solution.py:98
  48.3 11.2 %collective-permute-start.3 = (bf16[256,2,256]{2,0,1:T(8,128)(2,1)}, bf16[256,2,256]{2,0,1:T(8,128)(2,1)S(1)}, u32[]{:S(2)}, u32[]{:S(2)}) collective-permute-start(bf16[256,2,256]{2,0,1:T(8,128)(2,1)} %collective-permute-done.1), channel_id=1, source_target_pairs={{0,4},{4,8},{8,12},{12,16},{16,20},{20,24},{24,28},{28,0},{1,5},{5... | collective-permute-start | bytes 786440 | tf_op jit(solution)/shard_map/ppermute | solution.py:96
  53.7 16.4 %collective-permute-start.4 = (bf16[256,2,256]{2,0,1:T(8,128)(2,1)S(1)}, bf16[256,2,256]{2,0,1:T(8,128)(2,1)S(1)}, u32[]{:S(2)}, u32[]{:S(2)}) collective-permute-start(bf16[256,2,256]{2,0,1:T(8,128)(2,1)S(1)} %collective-permute-done.2), channel_id=1, source_target_pairs={{0,28},{4,0},{8,4},{12,8},{16,12},{20,16},{24,20},{28,24},{1,29},{... | collective-permute-start | bytes 786440 | tf_op jit(solution)/shard_map/ppermute | solution.py:98
  59.6 10.2 %collective-permute-start.5 = (bf16[256,2,256]{2,0,1:T(8,128)(2,1)S(1)}, bf16[256,2,256]{2,0,1:T(8,128)(2,1)S(1)}, u32[]{:S(2)}, u32[]{:S(2)}) collective-permute-start(bf16[256,2,256]{2,0,1:T(8,128)(2,1)S(1)} %collective-permute-done.3), channel_id=1, source_target_pairs={{0,4},{4,8},{8,12},{12,16},{16,20},{20,24},{24,28},{28,0},{1,5},{5... | collective-permute-start | bytes 786440 | tf_op jit(solution)/shard_map/ppermute | solution.py:96
  69.8 11.2 %collective-permute-start.6 = (bf16[256,2,256]{2,0,1:T(8,128)(2,1)S(1)}, bf16[256,2,256]{2,0,1:T(8,128)(2,1)S(1)}, u32[]{:S(2)}, u32[]{:S(2)}) collective-permute-start(bf16[256,2,256]{2,0,1:T(8,128)(2,1)S(1)} %collective-permute-done.5), channel_id=1, source_target_pairs={{0,4},{4,8},{8,12},{12,16},{16,20},{20,24},{24,28},{28,0},{1,5},{5... | collective-permute-start | bytes 786440 | tf_op jit(solution)/shard_map/ppermute | solution.py:96
  70.3 10.9 %copy-start.2 = (bf16[4,384,128]{1,2,0:T(8,128)(2,1)S(1)}, bf16[4,384,128]{1,2,0:T(8,128)(2,1)}, u32[]{:S(2)}) copy-start(bf16[4,384,128]{1,2,0:T(8,128)(2,1)} %get-tuple-element.51) | copy-start | bytes 1179652
  82.1 1.4 copy-start.9
  82.1 78.2 %copy-start.6 = (f32[32,2,512]{2,1,0:T(2,128)S(1)}, f32[32,2,512]{2,1,0:T(2,128)}, u32[]{:S(2)}) copy-start(f32[32,2,512]{2,1,0:T(2,128)} %param.20) | copy-start | bytes 393220
  83.4 78.7 %copy-start.3 = (f32[256,2,512]{2,1,0:T(2,128)S(1)}, f32[256,2,512]{2,1,0:T(2,128)}, u32[]{:S(2)}) copy-start(f32[256,2,512]{2,1,0:T(2,128)} %param.21) | copy-start | bytes 3145732
  83.5 119.9 %all-gather.3.cloned.1.call-start = ((), (), s32[]{:S(2)}) async-start(), calls=%async_computation | async-start | bytes 1179648 | tf_op jit(solution)/shard_map/all_gather | solution.py:134
  162.1 118.9 %all-gather.5.cloned.1.call-start = ((), (), s32[]{:S(2)}) async-start(), calls=%async_computation.1 | async-start | bytes 4718592 | tf_op jit(solution)/shard_map/all_gather | solution.py:138
Sparse Core Ops, SparseCore 0:
  83.6 76.6 all-reduce.2
  163.0 40.0 all-gather.2
  207.0 74.0 all-gather.4
